TPU v7x, 512 devices: a whole 4x4x16 slice. The times are simulated.
512 devices in a mesh: sp: 64 (over z, y), tp: 8 (over x, core).
Axes of the slice: x: 4, y: 4, z: 16, core: 2. Of those that a mesh axis runs over, the one named last changes fastest.
Arguments:
- queries: bfloat16 [16384, 1024], P('sp', 'tp'), may hold values from -6 to 6
- keys: bfloat16 [16384, 512], P('sp', 'tp'), may hold values from -6 to 6
- values: bfloat16 [16384, 512], P('sp', 'tp'), may hold values from -6 to 6
- q_gain: float32 [64], replicated, may hold values from 1.6 to 4.5
- key_norm_gain: float32 [64], replicated, may hold values from 1.6 to 4.5
- out_weight: bfloat16 [1024, 2048], P('tp'), may hold values from -0.1875 to 0.1875
- residual: bfloat16 [16384, 2048], P('sp'), may hold values from -6 to 6
- ln1_gain: float32 [2048], replicated, may hold values from 0.1 to 1.9
- ln1_bias: float32 [2048], replicated, may hold values from -3 to 3
- up_weight: bfloat16 [2048, 8192], P('sp', 'tp'), may hold values from -0.125 to 0.125
- down_weight: bfloat16 [8192, 2048], P('tp', 'sp'), may hold values from -0.0625 to 0.0625
- ln2_gain: float32 [2048], replicated, may hold values from 0.1 to 1.9
- ln2_bias: float32 [2048], replicated, may hold values from -3 to 3
Outputs:
- encoded: bfloat16 [16384, 2048], P('sp', 'tp')
All inputs are finite; a program needn't handle non-finite values.
Results may differ from a plain program's by a relative error of at most 0.014.
Values may be sent and summed in bfloat16 or wider, within the bound.
A program may use at most 64 MiB of HBM per device.

v0:
```python
import math
import jax
import jax.numpy as jnp
from jax import lax
from jax.sharding import PartitionSpec as P

D = 2048
HEAD_SIZE = 64
GRID_W = 64
ALPHA = 8.0**0.25
ROTARY_BASE = 10000.0
RMS_EPSILON = 1e-06
NORM_EPSILON = 1e-05


def turned_gather(arrays, axis, dims):
    turned = [jnp.moveaxis(a, dim, 0) for a, dim in zip(arrays, dims)]
    both = jnp.concatenate([t.reshape(len(t), -1) for t in turned], axis=1)
    out, at, finished = (lax.all_gather(both, axis, axis=0, tiled=True), 0, [])
    for t, dim in zip(turned, dims):
        piece = out[:, at : at + t[0].size].reshape(-1, *t.shape[1:])
        finished.append(jnp.moveaxis(piece, 0, dim))
        at += t[0].size
    return tuple(finished)


def side_by_side(arrays, axis, dim, along):
    widths = [a.shape[along] for a in arrays]
    both = jnp.concatenate(arrays, axis=along)
    out = lax.all_gather(both, axis, axis=dim, tiled=True)
    return tuple(jnp.split(out, [sum(widths[:k]) for k in range(1, len(widths))], axis=along))


def split_up(array, dim, devices):
    before, after = (array.shape[:dim], array.shape[dim + 1 :])
    return jnp.moveaxis(array.reshape(*before, devices, -1, *after), dim, 0)


def sent_and_summed(array, axis, dim):
    devices = lax.axis_size(axis)
    blocks = lax.all_to_all(split_up(array, dim, devices), axis, 0, 0, tiled=True)
    return jnp.sum(blocks.astype(jnp.float32), axis=0)


def from_everyone(array, axis):
    devices = lax.axis_size(axis)
    return lax.all_to_all(
        jnp.broadcast_to(array[None], (devices, *array.shape)), axis, 0, 0, tiled=True
    )


def over_copies(array, axis):
    everything = from_everyone(array, axis)
    return jnp.sum(everything, axis=0)


def in_one(arrays, axis):
    ends = [0]
    for a in arrays:
        ends.append(ends[-1] + a.size)
    running = over_copies(jnp.concatenate([a.ravel() for a in arrays]), axis)
    return tuple((running[b:e].reshape(a.shape) for a, b, e in zip(arrays, ends, ends[1:])))


def laid_out(blocks, dim):
    lengths = list(blocks.shape[1:])
    lengths[dim] *= blocks.shape[0]
    return jnp.moveaxis(blocks, 0, dim).reshape(lengths)


def gathered_copies(array, axis, dim):
    return laid_out(from_everyone(array, axis), dim)


def rotate_grid(heads_in, grid_places):
    half_dim = heads_in.shape[-1] // 2
    quarter = half_dim // 2
    inverse = ROTARY_BASE ** (-jnp.arange(quarter, dtype=jnp.float32) / quarter)

    def spin(segment, coords):
        angles = coords.astype(jnp.float32)[:, None] * inverse[None, :]
        cos_val = jnp.cos(angles)[:, None, :]
        sin_val = jnp.sin(angles)[:, None, :]
        lead_half = segment[..., :quarter]
        tail_half = segment[..., quarter:]
        return jnp.concatenate(
            [lead_half * cos_val - tail_half * sin_val, tail_half * cos_val + lead_half * sin_val],
            -1,
        )

    return jnp.concatenate(
        [
            spin(heads_in[..., :half_dim], grid_places // GRID_W),
            spin(heads_in[..., half_dim:], grid_places % GRID_W),
        ],
        -1,
    )


def prepare_inputs(heads_in, gain_vec, grid_places, factor):
    values32 = heads_in.astype(jnp.float32)
    normed = (
        values32
        * lax.rsqrt(jnp.mean(values32 * values32, -1, keepdims=True) + RMS_EPSILON)
        * gain_vec
    )
    return (rotate_grid(normed, grid_places) * factor).astype(jnp.bfloat16)


def finish_norm(pre_norm, stats, gain_vec, bias_vec):
    row_mean = stats[0][:, None] / D
    spread = stats[1][:, None] / D - row_mean * row_mean
    return (pre_norm - row_mean) * lax.rsqrt(spread + NORM_EPSILON) * gain_vec + bias_vec


def take_cols(array_in, col_start, col_width):
    return lax.dynamic_slice_in_dim(array_in, col_start, col_width, array_in.ndim - 1)


def local(
    queries,
    keys,
    values,
    q_gain,
    key_norm_gain,
    out_weight,
    residual,
    ln1_gain,
    ln1_bias,
    up_weight,
    down_weight,
    ln2_gain,
    ln2_bias,
):
    tok_rows = queries.shape[0]
    up_whole, down_whole = turned_gather((up_weight, down_weight), "sp", (0, 1))
    grid_places = lax.axis_index("sp") * tok_rows + jnp.arange(tok_rows, dtype=jnp.int32)
    kv_heads = keys.shape[1] // HEAD_SIZE
    q_count = queries.shape[1] // HEAD_SIZE
    group_count_size = q_count // kv_heads
    query_head_rows = prepare_inputs(
        queries.reshape(tok_rows, q_count, HEAD_SIZE), q_gain, grid_places, HEAD_SIZE ** (-0.5)
    )
    q_grouped = query_head_rows.reshape(tok_rows, kv_heads, group_count_size, HEAD_SIZE)
    k_sent = prepare_inputs(
        keys.reshape(tok_rows, kv_heads, HEAD_SIZE), key_norm_gain, grid_places, 1.0
    ).reshape(tok_rows, kv_heads * HEAD_SIZE)
    initial = (
        jnp.full((kv_heads, group_count_size, tok_rows), -jnp.inf, jnp.float32),
        jnp.zeros((kv_heads, group_count_size, tok_rows), jnp.float32),
        jnp.zeros((tok_rows, kv_heads, group_count_size, HEAD_SIZE), jnp.float32),
    )
    key_piece, value_piece = side_by_side((k_sent, values), "sp", 0, 1)
    key_count = key_piece.shape[0]
    block_len = math.gcd(key_count, 2048)
    key_blocks = key_piece.reshape(key_count // block_len, block_len, kv_heads, HEAD_SIZE)
    value_blocks = value_piece.reshape(key_count // block_len, block_len, kv_heads, HEAD_SIZE)

    def advance(state_in, blocks):
        maxima, totals, accumulated = state_in
        scores = jnp.einsum(
            "qhgd,khd->hgqk", q_grouped, blocks[0], preferred_element_type=jnp.float32
        )
        new_max = jnp.maximum(maxima, jnp.max(scores, -1))
        factor = jnp.exp(maxima - new_max)
        weights = jnp.exp(scores - new_max[..., None])
        totals = totals * factor + jnp.sum(weights, -1)
        update = jnp.einsum(
            "hgqk,khd->qhgd",
            weights.astype(jnp.bfloat16),
            blocks[1],
            preferred_element_type=jnp.float32,
        )
        accumulated = accumulated * jnp.transpose(factor, (2, 0, 1))[..., None] + update
        return ((new_max, totals, accumulated), None)

    state_out, unused = lax.scan(advance, initial, (key_blocks, value_blocks))
    maxima, totals, accumulated = state_out
    attended = (
        (accumulated / jnp.transpose(totals, (2, 0, 1))[..., None])
        .reshape(tok_rows, q_count * HEAD_SIZE)
        .astype(jnp.bfloat16)
    )
    partial_value = jnp.dot(attended, out_weight, preferred_element_type=jnp.float32)
    col_width = D // lax.axis_size("tp")
    col_start = lax.axis_index("tp") * col_width
    mixed_cols = sent_and_summed(partial_value.astype(jnp.bfloat16), "tp", 1)
    pre_norm = ALPHA * take_cols(residual, col_start, col_width).astype(jnp.float32) + mixed_cols
    stats = in_one((jnp.sum(pre_norm, -1), jnp.sum(pre_norm * pre_norm, -1)), "tp")
    normed_own = finish_norm(
        pre_norm,
        stats,
        take_cols(ln1_gain, col_start, col_width),
        take_cols(ln1_bias, col_start, col_width),
    ).astype(jnp.bfloat16)
    full_rows = gathered_copies(normed_own, "tp", 1)
    up_acts = jnp.dot(full_rows, up_whole, preferred_element_type=jnp.float32)
    hidden = jnp.square(jnp.maximum(up_acts, 0.0)).astype(jnp.bfloat16)
    partial_ffn = jnp.dot(hidden, down_whole, preferred_element_type=jnp.float32)
    ffn_cols = sent_and_summed(partial_ffn.astype(jnp.bfloat16), "tp", 1)
    second = ALPHA * normed_own.astype(jnp.float32) + ffn_cols
    stats_two = in_one((jnp.sum(second, -1), jnp.sum(second * second, -1)), "tp")
    return finish_norm(
        second,
        stats_two,
        take_cols(ln2_gain, col_start, col_width),
        take_cols(ln2_bias, col_start, col_width),
    ).astype(jnp.bfloat16)


def solution(mesh):
    return jax.shard_map(
        local,
        mesh=mesh,
        in_specs=(
            P("sp", "tp"),
            P("sp", "tp"),
            P("sp", "tp"),
            P(),
            P(),
            P("tp", None),
            P("sp", None),
            P(),
            P(),
            P("sp", "tp"),
            P("tp", "sp"),
            P(),
            P(),
        ),
        out_specs=P("sp", "tp"),
        check_vma=False,
    )
```

profile of v0, /device:TPU:1, one launch (start us, length us, event | category | flops | bytes accessed | tf_op | source)
XLA Modules:
  0.0 357.5 jit_solution(9664578682468562471)
XLA Ops:
  6.6 0.8 fusion.43
  7.4 0.8 fusion.45
  8.8 0.8 constant_dynamic-update-slice_fusion
  9.6 0.6 copy-done.2
  10.3 1.5 pad_maximum_fusion
  12.1 0.9 copy.36
  13.1 0.7 multiply_multiply_fusion
  13.9 137.4 %all-gather.3.cloned.1.call-done = bf16[16384,128]{0,1:T(8,128)(2,1)} async-done(((bf16[256,128]{0,1:T(8,128)(2,1)}), bf16[16384,128]{0,1:T(8,128)(2,1)}) %all-gather.3.cloned.1.call-update) | async-done | bytes 4194320 | tf_op jit(solution)/shard_map/all_gather | solution.py:30
  151.3 2.6 fusion.67
  153.9 1.2 copy.53
  155.1 1.2 copy.37
  156.2 1.2 copy.54
  157.4 2.5 copy.38
  159.9 54.9 %while.15 = (s32[]{:T(128)}, f32[1,2,256]{2,1,0:T(2,128)S(1)}, f32[1,2,256]{2,1,0:T(2,128)S(1)}, f32[256,1,2,64]{0,3,2,1:T(8,128)S(1)}, bf16[8,2048,1,64]{1,3,2,...) while((s32[]{:T(128)}, f32[1,2,256]{2,1,0:T(2,128)S(1)}, ...), condition=%wide.region_5.6_spmd.clone, body=%wide.region_2.5_spmd.clone.sunk | while | flops 273779712 | bytes 30245512 | solution.py:177
  159.9 2.7 bitcast_reduce_fusion.2
  162.7 3.2 fusion.80
  166.8 2.7 bitcast_reduce_fusion.2
  169.5 3.2 fusion.80
  173.6 2.7 bitcast_reduce_fusion.2
  176.4 3.2 fusion.80
  180.5 2.7 bitcast_reduce_fusion.2
  183.2 3.2 fusion.80
  187.4 2.7 bitcast_reduce_fusion.2
  190.1 3.2 fusion.80
  194.2 2.7 bitcast_reduce_fusion.2
  197.0 3.2 fusion.80
  201.1 2.7 bitcast_reduce_fusion.2
  203.9 3.2 fusion.80
  208.0 2.7 bitcast_reduce_fusion.2
  210.7 3.2 fusion.80
  215.4 1.1 copy.58
  216.5 14.5 %all-to-all-start = ((bf16[8,256,256]{2,1,0:T(8,128)(2,1)}), bf16[8,256,256]{2,1,0:T(8,128)(2,1)S(1)}, u32[]{:S(2)}, u32[]{:S(2)}) async-start(bf16[8,256,256]{2,1,0:T(8,128)(2,1)} %bitcast.113), calls=%async_computation | async-start | bytes 2097152 | tf_op jit(solution)/shard_map/all_to_all | solution.py:41
  231.0 15.0 %all-to-all-done = bf16[8,256,256]{2,1,0:T(8,128)(2,1)S(1)} async-done(((bf16[8,256,256]{2,1,0:T(8,128)(2,1)}), bf16[8,256,256]{2,1,0:T(8,128)(2,1)S(1)}, u32[]{:S(2)}, u32[]{:S(2)}) %all-to-all-start) | async-done | bytes 1048608 | tf_op jit(solution)/shard_map/all_to_all | solution.py:41
  246.1 1.1 fusion.46
  247.8 4.2 %all-to-all-start.1 = ((f32[8,1,512]{2,1,0:T(1,128)}), f32[8,1,512]{2,1,0:T(1,128)S(1)}, u32[]{:S(2)}, u32[]{:S(2)}) async-start(f32[8,1,512]{2,1,0:T(1,128)} %broadcast_in_dim.15), calls=%async_computation.1 | async-start | bytes 32768 | tf_op jit(solution)/shard_map/all_to_all | solution.py:47
  252.0 0.8 dynamic_slice.23
  252.7 0.8 dynamic_slice.24
  253.5 3.2 all-to-all-done.1
  256.8 1.1 add_convert_fusion.1
  258.0 18.0 %all_to_all.27 = bf16[8,256,256]{1,2,0:T(8,128)(2,1)S(1)} all-to-all(bf16[8,256,256]{1,2,0:T(8,128)(2,1)S(1)} %broadcast_in_dim.16), channel_id=1, replica_groups=mesh['sp'=64,'tp'=8] {'tp'}, dimensions={0} | all-to-all | bytes 2097152 | tf_op jit(solution)/shard_map/all_to_all | solution.py:47
  276.1 30.5 %all-gather.5.cloned.1.call-done = bf16[2048,2048]{1,0:T(8,128)(2,1)} async-done(((bf16[32,2048]{1,0:T(8,128)(2,1)}), bf16[2048,2048]{1,0:T(8,128)(2,1)}) %all-gather.5.cloned.1.call-update) | async-done | bytes 8388624 | tf_op jit(solution)/shard_map/all_gather | solution.py:19
  306.6 5.8 %fusion.26 = bf16[256,2048]{1,0:T(8,128)(2,1)S(1)} fusion(bf16[2048,2048]{1,0:T(8,128)(2,1)} %all-gather.5.cloned.1.call-done, bf16[256,2048]{0,1:T(8,128)(2,1)S(1)} %bitcast.144), kind=kOutput, calls=%fused_computation.30 | convolution fusion | flops 2148794368 | bytes 10485760 | tf_op jit(solution)/shard_map/dot_general | solution.py:199
  312.5 27.4 %all_to_all.28 = bf16[8,256,256]{2,1,0:T(8,128)(2,1)S(1)} all-to-all(bf16[8,256,256]{2,1,0:T(8,128)(2,1)S(1)} %bitcast.141), channel_id=1, replica_groups=mesh['sp'=64,'tp'=8] {'tp'}, dimensions={0} | all-to-all | bytes 2097152 | tf_op jit(solution)/shard_map/all_to_all | solution.py:41
  340.9 4.3 %all-to-all-start.4 = ((f32[8,1,512]{2,1,0:T(1,128)}), f32[8,1,512]{2,1,0:T(1,128)S(1)}, u32[]{:S(2)}, u32[]{:S(2)}) async-start(f32[8,1,512]{2,1,0:T(1,128)} %broadcast_in_dim.17), calls=%async_computation.4 | async-start | bytes 32768 | tf_op jit(solution)/shard_map/all_to_all | solution.py:47
  345.1 0.8 dynamic_slice.25
  345.9 0.8 dynamic_slice.26
  346.7 3.2 all-to-all-done.4
  349.9 0.8 add_convert_fusion
  (86 shorter events, 10.6 us)
Async XLA Ops:
  6.5 208.4 %copy-start = (bf16[128,2048]{1,0:T(8,128)(2,1)S(1)}, bf16[128,2048]{1,0:T(8,128)(2,1)}, u32[]{:S(2)}) copy-start(bf16[128,2048]{1,0:T(8,128)(2,1)} %param.20) | copy-start | bytes 1572868
  6.5 144.7 %all-gather.3.cloned.1.call-start = ((), (), s32[]{:S(2)}) async-start(), calls=%async_computation.5 | async-start | bytes 4259840 | tf_op jit(solution)/shard_map/all_gather | solution.py:30
  9.6 0.6 copy-start.2
  10.2 296.4 %all-gather.5.cloned.1.call-start = ((), (), s32[]{:S(2)}) async-start(), calls=%async_computation.6 | async-start | bytes 8519680 | tf_op jit(solution)/shard_map/all_gather | solution.py:19
  162.6 3.5 copy-start.1
  169.5 3.5 copy-start.1
  176.4 3.5 copy-start.1
  183.2 3.6 copy-start.1
  190.1 3.5 copy-start.1
  197.0 3.6 copy-start.1
  203.8 3.5 copy-start.1
  210.7 3.6 copy-start.1
  216.5 29.5 %all-to-all-start = ((bf16[8,256,256]{2,1,0:T(8,128)(2,1)}), bf16[8,256,256]{2,1,0:T(8,128)(2,1)S(1)}, u32[]{:S(2)}, u32[]{:S(2)}) async-start(bf16[8,256,256]{2,1,0:T(8,128)(2,1)} %bitcast.113), calls=%async_computation | async-start | bytes 2097152 | tf_op jit(solution)/shard_map/all_to_all | solution.py:41
  247.8 8.9 %all-to-all-start.1 = ((f32[8,1,512]{2,1,0:T(1,128)}), f32[8,1,512]{2,1,0:T(1,128)S(1)}, u32[]{:S(2)}, u32[]{:S(2)}) async-start(f32[8,1,512]{2,1,0:T(1,128)} %broadcast_in_dim.15), calls=%async_computation.1 | async-start | bytes 32768 | tf_op jit(solution)/shard_map/all_to_all | solution.py:47
  340.9 9.0 %all-to-all-start.4 = ((f32[8,1,512]{2,1,0:T(1,128)}), f32[8,1,512]{2,1,0:T(1,128)S(1)}, u32[]{:S(2)}, u32[]{:S(2)}) async-start(f32[8,1,512]{2,1,0:T(1,128)} %broadcast_in_dim.17), calls=%async_computation.4 | async-start | bytes 32768 | tf_op jit(solution)/shard_map/all_to_all | solution.py:47
Sparse Core Ops, SparseCore 0:
  10.4 140.8 all-gather.2
  154.2 152.3 all-gather.4
where the time goes:
time: 358 us; the launch traced here: 357 us
  waiting for transfers between devices  189 us (53%)
  matrix products  53.7 us (15%)
  blocking collectives  45.5 us (13%)
  starting transfers between devices  23 us (6%)
  local copies, waits for them, and re-layouts  19.1 us (5%)
  between operations  13.6 us (4%)
  other arithmetic  13 us (4%)
    all_gather x1, waiting for transfers between devices, side_by_side(): out = lax.all_gather(both, axis, axis=dim, tiled=True)  137 us
    all_gather x1, waiting for transfers between devices, turned_gather(): out, at, finished = (lax.all_gather(both, axis, axis=0, tiled=True), 0, [])  30.5 us
    all_to_all x1, blocking collectives, sent_and_summed(): lax.all_to_all(split_up(array, dim, devices), axis, 0, 0, tiled=True)  27.4 us
    dot_general x8, matrix products, advance(): jnp.einsum('hgqk,khd->qhgd', weights.astype(jnp.bfloat16), blocks[1], pre...  25.7 us
    dot_general x8, matrix products, advance(): jnp.einsum('qhgd,khd->hgqk', q_grouped, blocks[0], preferred_element_type...  21.7 us
    all_to_all x1, blocking collectives, from_everyone(): lax.all_to_all(jnp.broadcast_to(array[None], (devices, *array.shape)), ax...  18 us
    all_to_all x1, waiting for transfers between devices, sent_and_summed(): lax.all_to_all(split_up(array, dim, devices), axis, 0, 0, tiled=True)  15 us
    all_to_all x1, starting transfers between devices, sent_and_summed(): lax.all_to_all(split_up(array, dim, devices), axis, 0, 0, tiled=True)  14.5 us
  transfers between devices with their start and end apart: 5, of which 5 were waited for; matrix products, arithmetic and copies ran while one was open for 20% of the time, Pallas kernels for 0%

commit v1 on v0

--- a/solution.py
+++ b/solution.py
@@ -16,7 +16,13 @@
 def turned_gather(arrays, axis, dims):
     turned = [jnp.moveaxis(a, dim, 0) for a, dim in zip(arrays, dims)]
     both = jnp.concatenate([t.reshape(len(t), -1) for t in turned], axis=1)
-    out, at, finished = (lax.all_gather(both, axis, axis=0, tiled=True), 0, [])
+    keep_up_bars = lambda content, across, join_dim: jnp.concatenate(
+        lax.all_to_all(
+            jnp.stack([content for _ in range(lax.psum(1, across))], axis=0), across, 0, 0
+        ),
+        join_dim,
+    )
+    out, at, finished = (keep_up_bars(both, axis, 0), 0, [])
     for t, dim in zip(turned, dims):
         piece = out[:, at : at + t[0].size].reshape(-1, *t.shape[1:])
         finished.append(jnp.moveaxis(piece, 0, dim))

time: 358 us -> 708 us (1.98)
  blocking collectives: 45.5 us -> 397 us
  other arithmetic: 13 us -> 30.2 us
  waiting for transfers between devices: 189 us -> 175 us
  matrix products: 53.7 us -> 41.5 us
    all_to_all x1, blocking collectives: 18 us -> 373 us  [turned_gather(): lax.all_to_all(jnp.stack([content for _ in range(lax.psum(1, across))], a...]
    all_gather x1 -> x0, waiting for transfers between devices: 30.5 us -> none  [turned_gather(): out, at, finished = (lax.all_gather(both, axis, axis=0, tiled=True), 0, [])]
    reduce_sum x8, other arithmetic: 4.52 us -> 23.2 us  [advance(): totals = totals * factor + jnp.sum(weights, -1)]
    all_to_all x2 -> x3, waiting for transfers between devices: 6.38 us -> 21.3 us  [from_everyone(): lax.all_to_all(jnp.broadcast_to(array[None], (devices, *array.shape)), ax...]
    dot_general x8, matrix products: 25.7 us -> 13.9 us  [advance(): jnp.einsum('hgqk,khd->qhgd', weights.astype(jnp.bfloat16), blocks[1], pre...]
  transfers between devices with their start and end apart: 5 -> 5, of which waited for: 5 -> 5; matrix products, arithmetic and copies ran while one was open for 20% -> 1% of each run, Pallas kernels for 0% -> 0%
where the time goes in v1:
time: 708 us; the launch traced here: 707 us
  blocking collectives  397 us (56%)
  waiting for transfers between devices  175 us (25%)
  matrix products  41.5 us (6%)
  other arithmetic  30.2 us (4%)
  starting transfers between devices  27.2 us (4%)
  local copies, waits for them, and re-layouts  22.6 us (3%)
  between operations  13.6 us (2%)
    all_to_all x1, blocking collectives, turned_gather(): lax.all_to_all(jnp.stack([content for _ in range(lax.psum(1, across))], a...  373 us
    all_gather x1, waiting for transfers between devices, side_by_side(): out = lax.all_gather(both, axis, axis=dim, tiled=True)  139 us
    all_to_all x1, blocking collectives, sent_and_summed(): lax.all_to_all(split_up(array, dim, devices), axis, 0, 0, tiled=True)  23.6 us
    reduce_sum x8, other arithmetic, advance(): totals = totals * factor + jnp.sum(weights, -1)  23.2 us
    dot_general x8, matrix products, advance(): jnp.einsum('qhgd,khd->hgqk', q_grouped, blocks[0], preferred_element_type...  21.3 us
    all_to_all x3, waiting for transfers between devices, from_everyone(): lax.all_to_all(jnp.broadcast_to(array[None], (devices, *array.shape)), ax...  21.3 us
    all_to_all x1, waiting for transfers between devices, sent_and_summed(): lax.all_to_all(split_up(array, dim, devices), axis, 0, 0, tiled=True)  15 us
    all_to_all x1, starting transfers between devices, sent_and_summed(): lax.all_to_all(split_up(array, dim, devices), axis, 0, 0, tiled=True)  14.5 us
  transfers between devices with their start and end apart: 5, of which 5 were waited for; matrix products, arithmetic and copies ran while one was open for 1% of the time, Pallas kernels for 0%

profile of v1, /device:TPU:1, one launch (start us, length us, event | category | flops | bytes accessed | tf_op | source)
XLA Modules:
  0.0 707.3 jit_solution(16376542717463174036)
XLA Ops:
  10.3 0.9 copy.36
  12.3 139.0 %all-gather.2.cloned.1.call-done = bf16[16384,128]{0,1:T(8,128)(2,1)} async-done(((bf16[256,128]{0,1:T(8,128)(2,1)}), bf16[16384,128]{0,1:T(8,128)(2,1)}) %all-gather.2.cloned.1.call-update) | async-done | bytes 4194320 | tf_op jit(solution)/shard_map/all_gather | solution.py:36
  151.3 2.6 fusion.67
  153.9 1.2 copy.53
  155.1 1.2 copy.37
  156.3 1.2 copy.54
  157.4 2.5 copy.38
  159.9 63.0 %while.15 = (s32[]{:T(128)}, f32[1,2,256]{2,1,0:T(2,128)S(1)}, f32[1,2,256]{2,1,0:T(2,128)S(1)}, f32[256,1,2,64]{0,3,2,1:T(8,128)S(1)}, bf16[8,2048,1,64]{1,3,2,...) while((s32[]{:T(128)}, f32[1,2,256]{2,1,0:T(2,128)S(1)}, ...), condition=%wide.region_5.6_spmd.clone, body=%wide.region_2.5_spmd.clone.sunk | while | flops 273779712 | bytes 30245012 | solution.py:183
  159.9 2.7 bitcast_reduce_fusion.2
  162.6 2.9 fusion.79
  166.0 1.7 fusion.80
  167.8 2.7 bitcast_reduce_fusion.2
  170.5 2.9 fusion.79
  173.9 1.7 fusion.80
  175.7 2.7 bitcast_reduce_fusion.2
  178.4 2.9 fusion.79
  181.8 1.7 fusion.80
  183.6 2.7 bitcast_reduce_fusion.2
  186.2 2.9 fusion.79
  189.7 1.7 fusion.80
  191.4 2.7 bitcast_reduce_fusion.2
  194.1 2.9 fusion.79
  197.5 1.7 fusion.80
  199.3 2.7 bitcast_reduce_fusion.2
  202.0 2.9 fusion.79
  205.4 1.7 fusion.80
  207.2 2.7 bitcast_reduce_fusion.2
  209.9 2.9 fusion.79
  213.3 1.7 fusion.80
  215.0 2.7 bitcast_reduce_fusion.2
  217.7 2.9 fusion.79
  221.2 1.7 fusion.80
  223.4 1.1 copy.58
  224.5 14.5 %all-to-all-start = ((bf16[8,256,256]{2,1,0:T(8,128)(2,1)}), bf16[8,256,256]{2,1,0:T(8,128)(2,1)S(1)}, u32[]{:S(2)}, u32[]{:S(2)}) async-start(bf16[8,256,256]{2,1,0:T(8,128)(2,1)} %bitcast.114), calls=%async_computation | async-start | bytes 2097152 | tf_op jit(solution)/shard_map/all_to_all | solution.py:47
  239.0 15.0 %all-to-all-done = bf16[8,256,256]{2,1,0:T(8,128)(2,1)S(1)} async-done(((bf16[8,256,256]{2,1,0:T(8,128)(2,1)}), bf16[8,256,256]{2,1,0:T(8,128)(2,1)S(1)}, u32[]{:S(2)}, u32[]{:S(2)}) %all-to-all-start) | async-done | bytes 1048608 | tf_op jit(solution)/shard_map/all_to_all | solution.py:47
  254.1 1.1 fusion.46
  255.8 4.2 all-to-all-start.1
  261.5 3.2 all-to-all-done.1
  264.7 1.0 add_convert_fusion.1
  265.9 1.1 broadcast_in_dim.16
  266.9 4.2 all-to-all-start.2
  271.1 15.0 %all-to-all-done.2 = bf16[8,256,256]{1,2,0:T(8,128)(2,1)S(1)} async-done(((bf16[8,256,256]{1,2,0:T(8,128)(2,1)}), bf16[8,256,256]{1,2,0:T(8,128)(2,1)S(1)}, u32[]{:S(2)}, u32[]{:S(2)}) %all-to-all-start.2) | async-done | bytes 1048608 | tf_op jit(solution)/shard_map/all_to_all | solution.py:53
  286.1 1.1 stack.2
  287.2 373.1 %all_to_all.32 = bf16[64,32,2048]{2,1,0:T(8,128)(2,1)} all-to-all(bf16[64,32,2048]{2,1,0:T(8,128)(2,1)S(1)} %stack.2), channel_id=1, replica_groups=mesh['sp'=64,'tp'=8] {'sp'}, dimensions={0} | all-to-all | bytes 16777216 | tf_op jit(solution)/shard_map/all_to_all | solution.py:20
  660.2 5.8 fusion.26
  666.1 23.6 %all_to_all.33 = bf16[8,256,256]{2,1,0:T(8,128)(2,1)S(1)} all-to-all(bf16[8,256,256]{2,1,0:T(8,128)(2,1)S(1)} %bitcast.143), channel_id=1, replica_groups=mesh['sp'=64,'tp'=8] {'tp'}, dimensions={0} | all-to-all | bytes 2097152 | tf_op jit(solution)/shard_map/all_to_all | solution.py:47
  690.7 4.3 all-to-all-start.5
  696.5 3.2 all-to-all-done.5
  (90 shorter events, 15.2 us)
Async XLA Ops:
  6.5 216.4 %copy-start = (bf16[128,2048]{1,0:T(8,128)(2,1)S(1)}, bf16[128,2048]{1,0:T(8,128)(2,1)}, u32[]{:S(2)}) copy-start(bf16[128,2048]{1,0:T(8,128)(2,1)} %param.20) | copy-start | bytes 1572868
  6.5 144.8 %all-gather.2.cloned.1.call-start = ((), (), s32[]{:S(2)}) async-start(), calls=%async_computation.6 | async-start | bytes 4259840 | tf_op jit(solution)/shard_map/all_gather | solution.py:36
  9.6 0.6 copy-start.2
  162.6 3.4 copy-start.1
  170.5 3.4 copy-start.1
  178.3 3.4 copy-start.1
  186.2 3.4 copy-start.1
  194.1 3.4 copy-start.1
  202.0 3.4 copy-start.1
  209.8 3.4 copy-start.1
  217.7 3.4 copy-start.1
  224.5 46.7 %copy-start.3 = (bf16[1024,32]{0,1:T(8,128)(2,1)S(1)}, bf16[1024,32]{0,1:T(8,128)(2,1)}, u32[]{:S(2)}) copy-start(bf16[1024,32]{0,1:T(8,128)(2,1)} %param.25) | copy-start | bytes 196612
  224.5 46.7 %copy-start.4 = (bf16[32,1024]{1,0:T(8,128)(2,1)S(1)}, bf16[32,1024]{1,0:T(8,128)(2,1)}, u32[]{:S(2)}) copy-start(bf16[32,1024]{1,0:T(8,128)(2,1)} %param.24) | copy-start | bytes 196612
  224.5 29.5 %all-to-all-start = ((bf16[8,256,256]{2,1,0:T(8,128)(2,1)}), bf16[8,256,256]{2,1,0:T(8,128)(2,1)S(1)}, u32[]{:S(2)}, u32[]{:S(2)}) async-start(bf16[8,256,256]{2,1,0:T(8,128)(2,1)} %bitcast.114), calls=%async_computation | async-start | bytes 2097152 | tf_op jit(solution)/shard_map/all_to_all | solution.py:47
  255.8 8.9 %all-to-all-start.1 = ((f32[8,1,512]{2,1,0:T(1,128)}), f32[8,1,512]{2,1,0:T(1,128)S(1)}, u32[]{:S(2)}, u32[]{:S(2)}) async-start(f32[8,1,512]{2,1,0:T(1,128)} %broadcast_in_dim.15), calls=%async_computation.1 | async-start | bytes 32768 | tf_op jit(solution)/shard_map/all_to_all | solution.py:53
  266.9 19.2 %all-to-all-start.2 = ((bf16[8,256,256]{1,2,0:T(8,128)(2,1)}), bf16[8,256,256]{1,2,0:T(8,128)(2,1)S(1)}, u32[]{:S(2)}, u32[]{:S(2)}) async-start(bf16[8,256,256]{1,2,0:T(8,128)(2,1)} %broadcast_in_dim.16), calls=%async_computation.2 | async-start | bytes 2097152 | tf_op jit(solution)/shard_map/all_to_all | solution.py:53
  690.7 9.0 %all-to-all-start.5 = ((f32[8,1,512]{2,1,0:T(1,128)}), f32[8,1,512]{2,1,0:T(1,128)S(1)}, u32[]{:S(2)}, u32[]{:S(2)}) async-start(f32[8,1,512]{2,1,0:T(1,128)} %broadcast_in_dim.17), calls=%async_computation.5 | async-start | bytes 32768 | tf_op jit(solution)/shard_map/all_to_all | solution.py:53
Sparse Core Ops, SparseCore 0:
  10.4 140.8 all-gather.1
